TPU v7x, 32 devices: a whole 2x2x4 slice. The times are simulated.
32 devices in a mesh: sp: 16 (over z, y, core), tp: 2 (over x).
Axes of the slice: x: 2, y: 2, z: 4, core: 2. Of those that a mesh axis runs over, the one named last changes fastest.
Arguments:
- queries: bfloat16 [8192, 1024], P('sp', 'tp'), may hold values from -260 to 260, as said below
- keys: bfloat16 [8192, 512], P('sp', 'tp'), may hold values from -8 to 8, as said below
- values: bfloat16 [8192, 512], P('sp', 'tp'), may hold values from -24 to 24
- doc_ids: int32 [8192], P('sp'), may hold values from 0 to 3, never falling along the last dimension, each value on 1 to 4096 neighbouring positions
- sink_logit: float32 [8], P('tp'), may hold values from 2 to 7
- residual_in: bfloat16 [8192, 2048], P(('sp', 'tp')), may hold values from -6 to 6
- w_out: bfloat16 [1024, 2048], replicated, may hold values from -0.375 to 0.375
- gain_one: float32 [2048], replicated, may hold values from 0.1 to 1.9
- w_gate: bfloat16 [2048, 5632], P('sp', 'tp'), may hold values from -0.125 to 0.125
- w_up: bfloat16 [2048, 5632], P('sp', 'tp'), may hold values from -0.125 to 0.125
- w_down: bfloat16 [5632, 2048], P('tp', 'sp'), may hold values from -0.078125 to 0.078125
- gain_two: float32 [2048], replicated, may hold values from 0.1 to 1.9
Outputs:
- layer_out: bfloat16 [8192, 2048], P(('sp', 'tp'))
Inputs may be any that keep to these rules, and one draw needn't show every extreme that they name: Real-valued projected queries. Real-valued projected keys. `doc_ids`: document numbers never fall along the sequence; each document is one run of positions.
All inputs are finite; a program needn't handle non-finite values.
Results may differ from a plain program's by a relative error of at most 0.012.
Values may be sent and summed in bfloat16 or wider, within the bound.
A program may use at most 128 MiB of HBM per device.

v0:
```python
import math
import jax
import jax.numpy as jnp
from jax import lax
from jax.sharding import PartitionSpec as P

HEAD = 128
HALF = 128
ALPHA = 2.0**0.5
EPS = 1e-05
NEGATIVE = -1e30


def shifted(value, axis, steps):
    count = lax.axis_size(axis)
    leading, last = (max(0, -steps), min(count, count - steps))
    return lax.ppermute(value, axis, [(source, source + steps) for source in range(leading, last)])


def layer_norm(values_in, gain):
    average = jnp.mean(values_in, -1, keepdims=True)
    centred = values_in - average
    variance = jnp.mean(centred * centred, -1, keepdims=True)
    return centred * lax.rsqrt(variance + EPS) * gain


def per_device(
    queries,
    keys,
    values,
    doc_ids,
    sink_logit,
    residual_in,
    w_out,
    gain_one,
    w_gate,
    w_up,
    w_down,
    gain_two,
):
    row_count = queries.shape[0]
    sp_size = lax.axis_size("sp")
    kv_local = keys.shape[1] // HEAD
    repeat = queries.shape[1] // keys.shape[1]
    lower = (keys[row_count - HALF :], values[row_count - HALF :], doc_ids[row_count - HALF :])
    upper = (keys[:HALF], values[:HALF], doc_ids[:HALF])
    before = shifted((lower[0], lower[1], lower[2]), "sp", 1)
    after = shifted((upper[0], upper[1], upper[2]), "sp", -1)
    keys_all = jnp.concatenate([before[0], keys, after[0]], 0)
    values_all = jnp.concatenate([before[1], values, after[1]], 0)
    docs_all = jnp.concatenate([before[2], doc_ids, after[2]], 0)
    first_pos = lax.axis_index("sp") * row_count
    block = math.gcd(512, row_count)
    span = block + 2 * HALF
    sinks = sink_logit.reshape(kv_local, repeat)

    def one_block(index):
        start = index * block
        query_blk = queries.reshape(block, kv_local, repeat, HEAD)
        key_blk = keys_all.reshape(span, kv_local, HEAD)
        value_blk = values_all.reshape(span, kv_local, HEAD)
        pos_query = first_pos + start + jnp.arange(block, dtype=jnp.int32)
        pos_key = first_pos + start - HALF + jnp.arange(span, dtype=jnp.int32)
        offset = pos_key[None, :] - pos_query[:, None]
        allowed = (jnp.abs(offset) <= HALF) & (docs_all[None, :] == doc_ids[:, None])
        allowed = allowed & (pos_key[None, :] >= 0) & (pos_key[None, :] < sp_size * row_count)
        scores = jnp.einsum(
            "qgrd,kgd->grqk", query_blk, key_blk, preferred_element_type=jnp.float32
        ) * HEAD ** (-0.5)
        scores = jnp.where(allowed[None, None], scores, NEGATIVE)
        top = jnp.maximum(jnp.max(scores, -1), sinks[:, :, None])
        weights = jnp.exp(scores - top[..., None])
        total = jnp.sum(weights, -1) + jnp.exp(sinks[:, :, None] - top)
        summed = jnp.einsum(
            "grqk,kgd->qgrd",
            weights.astype(jnp.bfloat16),
            value_blk,
            preferred_element_type=jnp.float32,
        )
        scaled = summed / jnp.transpose(total, (2, 0, 1))[..., None]
        return scaled.reshape(block, kv_local * repeat * HEAD).astype(jnp.bfloat16)

    attended = lax.map(one_block, jnp.arange(row_count // block, dtype=jnp.int32)).reshape(
        row_count, -1
    )
    token_rows = lax.all_to_all(attended, "tp", split_axis=0, concat_axis=1, tiled=True)
    mixed_rows = jnp.dot(token_rows, w_out, preferred_element_type=jnp.float32)
    pre_one = ALPHA * residual_in.astype(jnp.float32) + mixed_rows
    normed = layer_norm(pre_one, gain_one).astype(jnp.bfloat16)
    whole_rows = lax.all_gather(normed, "tp", axis=0, tiled=True)
    gate_whole, up_whole = (
        lax.all_gather(w_gate, "sp", axis=0, tiled=True),
        lax.all_gather(w_up, "sp", axis=0, tiled=True),
    )
    gate_part = jnp.dot(whole_rows, gate_whole, preferred_element_type=jnp.float32)
    up_part = jnp.dot(whole_rows, up_whole, preferred_element_type=jnp.float32)
    hidden = (jax.nn.silu(gate_part) * up_part).astype(jnp.bfloat16)
    down_terms = jnp.dot(
        hidden, lax.all_gather(w_down, "sp", axis=1, tiled=True), preferred_element_type=jnp.float32
    )
    rounded = lax.optimization_barrier(down_terms.astype(jnp.bfloat16)).astype(jnp.float32)
    down_rows = lax.psum_scatter(
        rounded.astype(jnp.bfloat16), "tp", scatter_dimension=0, tiled=True
    ).astype(jnp.float32)
    pre_two = ALPHA * normed.astype(jnp.float32) + down_rows
    return layer_norm(pre_two, gain_two).astype(jnp.bfloat16)


def solution(mesh):
    in_specs = (
        P("sp", "tp"),
        P("sp", "tp"),
        P("sp", "tp"),
        P("sp"),
        P("tp"),
        P(("sp", "tp"), None),
        P(),
        P(),
        P("sp", "tp"),
        P("sp", "tp"),
        P("tp", "sp"),
        P(),
    )
    out_specs = P(("sp", "tp"), None)
    return jax.shard_map(
        per_device, mesh=mesh, in_specs=in_specs, out_specs=out_specs, check_vma=False
    )
```

profile of v0, /device:TPU:0, one launch (start us, length us, event | category | flops | bytes accessed | tf_op | source)
XLA Modules:
  0.0 442.6 jit_solution(3270424816436045704)
XLA Ops:
  7.3 2.4 collective-permute-start.2
  9.7 1.3 collective-permute-start.3
  11.0 1.1 copy.17
  12.1 5.2 %collective-permute-start.4 = (bf16[128,256]{0,1:T(8,128)(2,1)S(1)}, bf16[128,256]{0,1:T(8,128)(2,1)S(1)}, u32[]{:S(2)}, u32[]{:S(2)}) collective-permute-start(bf16[128,256]{0,1:T(8,128)(2,1)S(1)} %get-tuple-element.21), channel_id=1, source_target_pairs={{0,2},{2,4},{4,6},{6,8},{8,10},{10,12},{12,14},{14,16},{16,18},{18... | collective-permute-start | bytes 196616 | tf_op jit(solution)/shard_map/ppermute | solution.py:17
  17.3 1.3 collective-permute-start.5
  19.5 4.3 collective-permute-start
  23.8 1.2 reshape.158
  25.1 1.3 collective-permute-start.1
  27.4 1.4 fusion.2
  29.0 1.4 fusion
  30.3 1.2 copy-done.1
  31.8 4.7 %divide_convert_fusion = bf16[512,2,2,128]{0,3,2,1:T(8,128)(2,1)S(1)} fusion(bf16[768,2,128,1]{0,2,3,1:T(8,128)(2,1)S(1)} %bitcast.47, f32[2,768,512,2]{2,1,3,0:T(8,128)} %copy-done.1, f32[2,2,512]{2,1,0:T(2,128)S(1)} %broadcast_maximum_fusion, pred[512,768]{0,1:T(8,128)(4,1)S(1)} %fusion.9, f32[512,2,2]{0,2,1:T(2,128)S(1)} %add_bitcast_fusion), kind=kOutput, calls=%fused_computation.21 | convolution fusion | flops 409468928 | bytes 7618560 | tf_op jit(solution)/shard_map/while/body/eval_jaxpr/grqk,kgd->qgrd/dot_general | solution.py:74
  36.8 10.8 %all_to_all.16 = bf16[2,256,512]{1,2,0:T(8,128)(2,1)S(1)} all-to-all(bf16[2,256,512]{1,2,0:T(8,128)(2,1)S(1)} %copy.23), channel_id=1, replica_groups=mesh['sp'=16,'tp'=2] {'tp'}, dimensions={0} | all-to-all | bytes 1048576 | tf_op jit(solution)/shard_map/all_to_all | solution.py:86
  47.6 3.6 fusion.25
  51.9 1.3 multiply_convert_fusion.2
  55.3 34.1 %all-gather.5.cloned.1.call-done = bf16[512,2048]{1,0:T(8,128)(2,1)} async-done(((bf16[256,2048]{1,0:T(8,128)(2,1)}), bf16[512,2048]{1,0:T(8,128)(2,1)}) %all-gather.5.cloned.1.call-update) | async-done | bytes 2097168 | tf_op jit(solution)/shard_map/all_gather | solution.py:90
  89.4 96.3 %all-gather.7.cloned.1.call-done = bf16[2048,2816]{1,0:T(8,128)(2,1)} async-done(((bf16[128,2816]{1,0:T(8,128)(2,1)}), bf16[2048,2816]{1,0:T(8,128)(2,1)}) %all-gather.7.cloned.1.call-update) | async-done | bytes 11534352 | tf_op jit(solution)/shard_map/all_gather | solution.py:92
  185.7 12.5 %fusion.26 = f32[512,2816]{1,0:T(8,128)} fusion(bf16[512,2048]{1,0:T(8,128)(2,1)} %all-gather.5.cloned.1.call-done, bf16[2048,2816]{1,0:T(8,128)(2,1)} %all-gather.7.cloned.1.call-done), kind=kOutput, calls=%fused_computation.44 | convolution fusion | flops 5905580032 | bytes 19398656 | tf_op jit(solution)/shard_map/dot_general | solution.py:95
  198.2 84.9 %all-gather.11.cloned.1.call-done = bf16[2816,2048]{1,0:T(8,128)(2,1)} async-done(((bf16[2816,128]{1,0:T(8,128)(2,1)}), bf16[2816,2048]{1,0:T(8,128)(2,1)}) %all-gather.11.cloned.1.call-update) | async-done | bytes 11534352 | tf_op jit(solution)/shard_map/all_gather | solution.py:99
  283.1 94.3 %all-gather.9.cloned.1.call-done = bf16[2048,2816]{1,0:T(8,128)(2,1)} async-done(((bf16[128,2816]{1,0:T(8,128)(2,1)}), bf16[2048,2816]{1,0:T(8,128)(2,1)}) %all-gather.9.cloned.1.call-update) | async-done | bytes 11534352 | tf_op jit(solution)/shard_map/all_gather | solution.py:93
  377.4 23.3 %convolution_convert_fusion = bf16[512,2048]{1,0:T(8,128)(2,1)} fusion(bf16[2816,2048]{1,0:T(8,128)(2,1)} %all-gather.11.cloned.1.call-done, f32[512,2816]{1,0:T(8,128)} %fusion.26, bf16[512,2048]{1,0:T(8,128)(2,1)} %all-gather.5.cloned.1.call-done, bf16[2048,2816]{1,0:T(8,128)(2,1)} %all-gather.9.cloned.1.call-done), kind=kOutput, calls=%fused_computation.8 | convolution fusion | flops 11820859392 | bytes 33030144 | tf_op jit(solution)/shard_map/dot_general | solution.py:98
  400.7 30.3 %reduce-scatter.2.cloned.1.call-done = bf16[256,2048]{1,0:T(8,128)(2,1)} async-done(((bf16[512,2048]{1,0:T(8,128)(2,1)}), bf16[256,2048]{1,0:T(8,128)(2,1)}) %reduce-scatter.2.cloned.1.call-update) | async-done | bytes 1048592 | tf_op jit(solution)/shard_map/reduce_scatter | solution.py:102
  431.0 1.9 fusion.6
  433.8 2.3 multiply_convert_fusion.1
  (53 shorter events, 6.9 us)
Async XLA Ops:
  6.5 19.9 %copy-start.5 = (s32[512]{0:T(512)S(1)}, s32[512]{0:T(512)}, u32[]{:S(2)}) copy-start(s32[512]{0:T(512)} %param.15) | copy-start | bytes 6148
  6.5 18.5 %copy-start.7 = (f32[4]{0:T(128)S(1)}, f32[4]{0:T(128)}, u32[]{:S(2)}) copy-start(f32[4]{0:T(128)} %param.16) | copy-start | bytes 52
  6.5 82.9 %all-gather.5.cloned.1.call-start = ((), (), s32[]{:S(2)}) async-start(), calls=%async_computation.2 | async-start | bytes 3145728 | tf_op jit(solution)/shard_map/all_gather | solution.py:90
  7.3 17.8 %collective-permute-start.2 = (s32[128]{0:T(128)S(1)}, s32[128]{0:T(128)S(1)}, u32[]{:S(2)}, u32[]{:S(2)}) collective-permute-start(s32[128]{0:T(128)S(1)} %get-tuple-element.25), channel_id=1, source_target_pairs={{0,2},{2,4},{4,6},{6,8},{8,10},{10,12},{12,14},{14,16},{16,18},{18... | collective-permute-start | bytes 1544 | tf_op jit(solution)/shard_map/ppermute | solution.py:17
  9.7 16.7 %collective-permute-start.3 = (s32[128]{0:T(128)S(1)}, s32[128]{0:T(128)S(1)}, u32[]{:S(2)}, u32[]{:S(2)}) collective-permute-start(s32[128]{0:T(128)S(1)} %get-tuple-element.26), channel_id=1, source_target_pairs={{2,0},{4,2},{6,4},{8,6},{10,8},{12,10},{14,12},{16,14},{18,16},{20... | collective-permute-start | bytes 1544 | tf_op jit(solution)/shard_map/ppermute | solution.py:17
  12.1 15.2 %collective-permute-start.4 = (bf16[128,256]{0,1:T(8,128)(2,1)S(1)}, bf16[128,256]{0,1:T(8,128)(2,1)S(1)}, u32[]{:S(2)}, u32[]{:S(2)}) collective-permute-start(bf16[128,256]{0,1:T(8,128)(2,1)S(1)} %get-tuple-element.21), channel_id=1, source_target_pairs={{0,2},{2,4},{4,6},{6,8},{8,10},{10,12},{12,14},{14,16},{16,18},{18... | collective-permute-start | bytes 196616 | tf_op jit(solution)/shard_map/ppermute | solution.py:17
  17.3 10.1 %collective-permute-start.5 = (bf16[128,256]{0,1:T(8,128)(2,1)S(1)}, bf16[128,256]{0,1:T(8,128)(2,1)S(1)}, u32[]{:S(2)}, u32[]{:S(2)}) collective-permute-start(bf16[128,256]{0,1:T(8,128)(2,1)S(1)} %get-tuple-element.22), channel_id=1, source_target_pairs={{2,0},{4,2},{6,4},{8,6},{10,8},{12,10},{14,12},{16,14},{18,16},{20... | collective-permute-start | bytes 196616 | tf_op jit(solution)/shard_map/ppermute | solution.py:17
  19.5 12.1 %collective-permute-start = (bf16[128,256]{1,0:T(8,128)(2,1)S(1)}, bf16[128,256]{1,0:T(8,128)(2,1)S(1)}, u32[]{:S(2)}, u32[]{:S(2)}) collective-permute-start(bf16[128,256]{1,0:T(8,128)(2,1)S(1)} %get-tuple-element.23), channel_id=1, source_target_pairs={{0,2},{2,4},{4,6},{6,8},{8,10},{10,12},{12,14},{14,16},{16,18},{18... | collective-permute-start | bytes 196616 | tf_op jit(solution)/shard_map/ppermute | solution.py:17
  25.1 6.5 %collective-permute-start.1 = (bf16[128,256]{1,0:T(8,128)(2,1)S(1)}, bf16[128,256]{1,0:T(8,128)(2,1)S(1)}, u32[]{:S(2)}, u32[]{:S(2)}) collective-permute-start(bf16[128,256]{1,0:T(8,128)(2,1)S(1)} %get-tuple-element.24), channel_id=1, source_target_pairs={{2,0},{4,2},{6,4},{8,6},{10,8},{12,10},{14,12},{16,14},{18,16},{20... | collective-permute-start | bytes 196616 | tf_op jit(solution)/shard_map/ppermute | solution.py:17
  28.9 2.6 copy-start.1
  29.0 2.7 copy-start.3
  36.5 11.1 %copy-start.2 = (bf16[256,2048]{1,0:T(8,128)(2,1)S(1)}, bf16[256,2048]{1,0:T(8,128)(2,1)}, u32[]{:S(2)}) copy-start(bf16[256,2048]{1,0:T(8,128)(2,1)} %param.17) | copy-start | bytes 3145732
  51.1 0.7 copy-start.4
  53.2 132.5 %all-gather.7.cloned.1.call-start = ((), (), s32[]{:S(2)}) async-start(), calls=%async_computation.3 | async-start | bytes 12255232 | tf_op jit(solution)/shard_map/all_gather | solution.py:92
  54.0 229.1 %all-gather.11.cloned.1.call-start = ((), (), s32[]{:S(2)}) async-start(), calls=%async_computation.5 | async-start | bytes 12255232 | tf_op jit(solution)/shard_map/all_gather | solution.py:99
  54.7 322.7 %all-gather.9.cloned.1.call-start = ((), (), s32[]{:S(2)}) async-start(), calls=%async_computation.4 | async-start | bytes 12255232 | tf_op jit(solution)/shard_map/all_gather | solution.py:93
  55.3 375.8 %reduce-scatter.2.cloned.1.call-start = ((), (), s32[]{:S(2)}) async-start(), calls=%async_computation.6 | async-start | bytes 3145728 | tf_op jit(solution)/shard_map/reduce_scatter | solution.py:102
  431.0 2.0 copy-start
  433.0 0.8 copy-start.6
Sparse Core Ops, SparseCore 0:
  53.3 36.0 all-gather.4
  91.7 93.9 all-gather.6
  187.9 95.1 all-gather.10
  285.2 92.1 all-gather.8
  400.8 30.1 reduce-scatter.1
where the time goes:
time: 443 us
  waiting for transfers between devices  342 us (77%)
  matrix products  45.5 us (10%)
  starting transfers between devices  15.8 us (4%)
  between operations  13.4 us (3%)
  blocking collectives  10.8 us (2%)
  other arithmetic  9.3 us (2%)
  local copies, waits for them, and re-layouts  5.92 us (1%)
    all_gather x1, waiting for transfers between devices, per_device(): lax.all_gather(w_gate, 'sp', axis=0, tiled=True)  96.3 us
    all_gather x1, waiting for transfers between devices, per_device(): lax.all_gather(w_up, 'sp', axis=0, tiled=True)  94.3 us
    all_gather x1, waiting for transfers between devices, per_device(): lax.all_gather(w_down, 'sp', axis=1, tiled=True)  84.9 us
    all_gather x1, waiting for transfers between devices, per_device(): whole_rows = lax.all_gather(normed, 'tp', axis=0, tiled=True)  34.1 us
    reduce_scatter x1, waiting for transfers between devices, per_device(): lax.psum_scatter(rounded.astype(jnp.bfloat16), 'tp', scatter_dimension=0,...  30.3 us
    dot_general x1, matrix products, per_device(): jnp.dot(hidden, lax.all_gather(w_down, 'sp', axis=1, tiled=True), preferr...  23.3 us
    ppermute x6, starting transfers between devices, shifted(): lax.ppermute(value, axis, [(source, source + steps) for source in range(l...  15.7 us
    dot_general x1, matrix products, per_device(): jnp.dot(whole_rows, gate_whole, preferred_element_type=jnp.float32)  12.5 us
  transfers between devices with their start and end apart: 11, of which 5 were waited for; matrix products, arithmetic and copies ran while one was open for 4% of the time, Pallas kernels for 0%

commit v1 on v0

--- a/solution.py
+++ b/solution.py
@@ -96,7 +96,9 @@
     up_part = jnp.dot(whole_rows, up_whole, preferred_element_type=jnp.float32)
     hidden = (jax.nn.silu(gate_part) * up_part).astype(jnp.bfloat16)
     down_terms = jnp.dot(
-        hidden, lax.all_gather(w_down, "sp", axis=1, tiled=True), preferred_element_type=jnp.float32
+        hidden,
+        jnp.concatenate(lax.all_gather(w_down, "sp"), axis=1),
+        preferred_element_type=jnp.float32,
     )
     rounded = lax.optimization_barrier(down_terms.astype(jnp.bfloat16)).astype(jnp.float32)
     down_rows = lax.psum_scatter(

time: 443 us -> 401 us (0.905)
  waiting for transfers between devices: 342 us -> 286 us
  local copies, waits for them, and re-layouts: 5.92 us -> 18.9 us
    all_gather x1, waiting for transfers between devices: 84.9 us -> 55.8 us  [per_device(): lax.all_gather(w_down, 'sp')]
    all_gather x1, waiting for transfers between devices: 34.1 us -> 17.7 us  [per_device(): whole_rows = lax.all_gather(normed, 'tp', axis=0, tiled=True)]
    reshape x0 -> x1, local copies, waits for them, and re-layouts: none -> 15.2 us  [per_device(): jnp.concatenate(lax.all_gather(w_down, 'sp'), axis=1)]
    all_gather x1, waiting for transfers between devices: 94.3 us -> 81.9 us  [per_device(): lax.all_gather(w_up, 'sp', axis=0, tiled=True)]
  transfers between devices with their start and end apart: 11 -> 11, of which waited for: 5 -> 6; matrix products, arithmetic and copies ran while one was open for 4% -> 11% of each run, Pallas kernels for 0% -> 0%
where the time goes in v1:
time: 401 us; the launch traced here: 400 us
  waiting for transfers between devices  286 us (71%)
  matrix products  46.7 us (12%)
  local copies, waits for them, and re-layouts  18.9 us (5%)
  starting transfers between devices  16.1 us (4%)
  between operations  13.4 us (3%)
  blocking collectives  9.82 us (2%)
  other arithmetic  9.31 us (2%)
    all_gather x1, waiting for transfers between devices, per_device(): lax.all_gather(w_gate, 'sp', axis=0, tiled=True)  96.3 us
    all_gather x1, waiting for transfers between devices, per_device(): lax.all_gather(w_up, 'sp', axis=0, tiled=True)  81.9 us
    all_gather x1, waiting for transfers between devices, per_device(): lax.all_gather(w_down, 'sp')  55.8 us
    reduce_scatter x1, waiting for transfers between devices, per_device(): lax.psum_scatter(rounded.astype(jnp.bfloat16), 'tp', scatter_dimension=0,...  30.2 us
    dot_general x1, matrix products, per_device(): jnp.dot(hidden, jnp.concatenate(lax.all_gather(w_down, 'sp'), axis=1), pr...  27.2 us
    all_gather x1, waiting for transfers between devices, per_device(): whole_rows = lax.all_gather(normed, 'tp', axis=0, tiled=True)  17.7 us
    ppermute x6, starting transfers between devices, shifted(): lax.ppermute(value, axis, [(source, source + steps) for source in range(l...  15.7 us
    reshape x1, local copies, waits for them, and re-layouts, per_device(): jnp.concatenate(lax.all_gather(w_down, 'sp'), axis=1)  15.2 us
  transfers between devices with their start and end apart: 11, of which 6 were waited for; matrix products, arithmetic and copies ran while one was open for 11% of the time, Pallas kernels for 0%

profile of v1, /device:TPU:0, one launch (start us, length us, event | category | flops | bytes accessed | tf_op | source)
XLA Modules:
  0.0 400.1 jit_solution(16999408934687025760)
XLA Ops:
  8.1 2.4 collective-permute-start.2
  10.5 1.3 collective-permute-start.3
  11.8 1.1 copy.25
  12.9 5.2 %collective-permute-start.4 = (bf16[128,256]{0,1:T(8,128)(2,1)S(1)}, bf16[128,256]{0,1:T(8,128)(2,1)S(1)}, u32[]{:S(2)}, u32[]{:S(2)}) collective-permute-start(bf16[128,256]{0,1:T(8,128)(2,1)S(1)} %get-tuple-element.21), channel_id=1, source_target_pairs={{0,2},{2,4},{4,6},{6,8},{8,10},{10,12},{12,14},{14,16},{16,18},{18... | collective-permute-start | bytes 196616 | tf_op jit(solution)/shard_map/ppermute | solution.py:17
  18.1 1.3 collective-permute-start.5
  20.3 4.3 %collective-permute-start = (bf16[128,256]{1,0:T(8,128)(2,1)S(1)}, bf16[128,256]{1,0:T(8,128)(2,1)S(1)}, u32[]{:S(2)}, u32[]{:S(2)}) collective-permute-start(bf16[128,256]{1,0:T(8,128)(2,1)S(1)} %get-tuple-element.23), channel_id=1, source_target_pairs={{0,2},{2,4},{4,6},{6,8},{8,10},{10,12},{12,14},{14,16},{16,18},{18... | collective-permute-start | bytes 196616 | tf_op jit(solution)/shard_map/ppermute | solution.py:17
  24.8 1.3 collective-permute-start.1
  27.1 2.1 collective-permute-done.1
  29.5 1.4 fusion.2
  31.0 1.4 fusion
  32.5 2.0 divide_convert_fusion
  34.7 9.8 %all_to_all.16 = bf16[2,256,512]{1,2,0:T(8,128)(2,1)S(1)} all-to-all(bf16[2,256,512]{1,2,0:T(8,128)(2,1)S(1)} %copy.31), channel_id=1, replica_groups=mesh['sp'=16,'tp'=2] {'tp'}, dimensions={0} | all-to-all | bytes 1048576 | tf_op jit(solution)/shard_map/all_to_all | solution.py:86
  44.5 3.6 fusion.25
  48.8 1.3 multiply_convert_fusion.2
  51.7 55.8 %all-gather.12.cloned.1.call-done = bf16[45056,128]{1,0:T(8,128)(2,1)} async-done(((bf16[2816,128]{1,0:T(8,128)(2,1)}), bf16[45056,128]{1,0:T(8,128)(2,1)}) %all-gather.12.cloned.1.call-update) | async-done | bytes 11534352 | tf_op jit(solution)/shard_map/all_gather | solution.py:100
  107.4 15.2 %copy.32 = bf16[2816,16,128]{0,2,1:T(8,128)(2,1)} copy(bf16[2816,16,128]{2,0,1:T(8,128)(2,1)} %bitcast.49) | data formatting | bytes 23068672 | tf_op jit(solution)/shard_map/reshape | solution.py:100
  122.6 17.7 %all-gather.6.cloned.1.call-done = bf16[512,2048]{1,0:T(8,128)(2,1)} async-done(((bf16[256,2048]{1,0:T(8,128)(2,1)}), bf16[512,2048]{1,0:T(8,128)(2,1)}) %all-gather.6.cloned.1.call-update) | async-done | bytes 2097168 | tf_op jit(solution)/shard_map/all_gather | solution.py:90
  140.3 96.3 %all-gather.8.cloned.1.call-done = bf16[2048,2816]{1,0:T(8,128)(2,1)} async-done(((bf16[128,2816]{1,0:T(8,128)(2,1)}), bf16[2048,2816]{1,0:T(8,128)(2,1)}) %all-gather.8.cloned.1.call-update) | async-done | bytes 11534352 | tf_op jit(solution)/shard_map/all_gather | solution.py:92
  236.6 12.5 %fusion.26 = f32[512,2816]{1,0:T(8,128)} fusion(bf16[512,2048]{1,0:T(8,128)(2,1)} %all-gather.6.cloned.1.call-done, bf16[2048,2816]{1,0:T(8,128)(2,1)} %all-gather.8.cloned.1.call-done), kind=kOutput, calls=%fused_computation.44 | convolution fusion | flops 5905580032 | bytes 19398656 | tf_op jit(solution)/shard_map/dot_general | solution.py:95
  249.1 81.9 %all-gather.10.cloned.1.call-done = bf16[2048,2816]{1,0:T(8,128)(2,1)} async-done(((bf16[128,2816]{1,0:T(8,128)(2,1)}), bf16[2048,2816]{1,0:T(8,128)(2,1)}) %all-gather.10.cloned.1.call-update) | async-done | bytes 11534352 | tf_op jit(solution)/shard_map/all_gather | solution.py:93
  331.0 27.2 %convolution_convert_fusion = bf16[512,2048]{1,0:T(8,128)(2,1)} fusion(bf16[2816,2048]{0,1:T(8,128)(2,1)} %bitcast.50, f32[512,2816]{1,0:T(8,128)} %fusion.26, bf16[512,2048]{1,0:T(8,128)(2,1)} %all-gather.6.cloned.1.call-done, bf16[2048,2816]{1,0:T(8,128)(2,1)} %all-gather.10.cloned.1.call-done), kind=kOutput, calls=%fused_computation.8 | convolution fusion | flops 11820859392 | bytes 33030144 | tf_op jit(solution)/shard_map/dot_general | solution.py:98
  358.3 30.2 %reduce-scatter.2.cloned.1.call-done = bf16[256,2048]{1,0:T(8,128)(2,1)} async-done(((bf16[512,2048]{1,0:T(8,128)(2,1)}), bf16[256,2048]{1,0:T(8,128)(2,1)}) %reduce-scatter.2.cloned.1.call-update) | async-done | bytes 1048592 | tf_op jit(solution)/shard_map/reduce_scatter | solution.py:104
  388.5 1.9 fusion.6
  391.3 2.3 multiply_convert_fusion.1
  (54 shorter events, 7.2 us)
Async XLA Ops:
  6.5 19.6 %copy-start.5 = (s32[512]{0:T(512)S(1)}, s32[512]{0:T(512)}, u32[]{:S(2)}) copy-start(s32[512]{0:T(512)} %param.15) | copy-start | bytes 6148
  6.5 22.7 %copy-start.2 = (bf16[512,256]{1,0:T(8,128)(2,1)S(1)}, bf16[512,256]{1,0:T(8,128)(2,1)}, u32[]{:S(2)}) copy-start(bf16[512,256]{1,0:T(8,128)(2,1)} %param.14) | copy-start | bytes 786436
  6.5 18.1 %copy-start.3 = (bf16[512,512]{1,0:T(8,128)(2,1)S(1)}, bf16[512,512]{1,0:T(8,128)(2,1)}, u32[]{:S(2)}) copy-start(bf16[512,512]{1,0:T(8,128)(2,1)} %param.12) | copy-start | bytes 1572868
  6.5 18.2 %copy-start.7 = (f32[4]{0:T(128)S(1)}, f32[4]{0:T(128)}, u32[]{:S(2)}) copy-start(f32[4]{0:T(128)} %param.16) | copy-start | bytes 52
  6.5 100.9 %all-gather.12.cloned.1.call-start = ((), (), s32[]{:S(2)}) async-start(), calls=%async_computation.6 | async-start | bytes 12255232 | tf_op jit(solution)/shard_map/all_gather | solution.py:100
  7.3 133.0 %all-gather.6.cloned.1.call-start = ((), (), s32[]{:S(2)}) async-start(), calls=%async_computation.2 | async-start | bytes 3145728 | tf_op jit(solution)/shard_map/all_gather | solution.py:90
  8.1 16.8 %collective-permute-start.2 = (s32[128]{0:T(128)S(1)}, s32[128]{0:T(128)S(1)}, u32[]{:S(2)}, u32[]{:S(2)}) collective-permute-start(s32[128]{0:T(128)S(1)} %get-tuple-element.25), channel_id=1, source_target_pairs={{0,2},{2,4},{4,6},{6,8},{8,10},{10,12},{12,14},{14,16},{16,18},{18... | collective-permute-start | bytes 1544 | tf_op jit(solution)/shard_map/ppermute | solution.py:17
  10.5 15.7 %collective-permute-start.3 = (s32[128]{0:T(128)S(1)}, s32[128]{0:T(128)S(1)}, u32[]{:S(2)}, u32[]{:S(2)}) collective-permute-start(s32[128]{0:T(128)S(1)} %get-tuple-element.26), channel_id=1, source_target_pairs={{2,0},{4,2},{6,4},{8,6},{10,8},{12,10},{14,12},{16,14},{18,16},{20... | collective-permute-start | bytes 1544 | tf_op jit(solution)/shard_map/ppermute | solution.py:17
  12.9 16.5 %collective-permute-start.4 = (bf16[128,256]{0,1:T(8,128)(2,1)S(1)}, bf16[128,256]{0,1:T(8,128)(2,1)S(1)}, u32[]{:S(2)}, u32[]{:S(2)}) collective-permute-start(bf16[128,256]{0,1:T(8,128)(2,1)S(1)} %get-tuple-element.21), channel_id=1, source_target_pairs={{0,2},{2,4},{4,6},{6,8},{8,10},{10,12},{12,14},{14,16},{16,18},{18... | collective-permute-start | bytes 196616 | tf_op jit(solution)/shard_map/ppermute | solution.py:17
  18.1 11.4 %collective-permute-start.5 = (bf16[128,256]{0,1:T(8,128)(2,1)S(1)}, bf16[128,256]{0,1:T(8,128)(2,1)S(1)}, u32[]{:S(2)}, u32[]{:S(2)}) collective-permute-start(bf16[128,256]{0,1:T(8,128)(2,1)S(1)} %get-tuple-element.22), channel_id=1, source_target_pairs={{2,0},{4,2},{6,4},{8,6},{10,8},{12,10},{14,12},{16,14},{18,16},{20... | collective-permute-start | bytes 196616 | tf_op jit(solution)/shard_map/ppermute | solution.py:17
  20.3 6.8 %collective-permute-start = (bf16[128,256]{1,0:T(8,128)(2,1)S(1)}, bf16[128,256]{1,0:T(8,128)(2,1)S(1)}, u32[]{:S(2)}, u32[]{:S(2)}) collective-permute-start(bf16[128,256]{1,0:T(8,128)(2,1)S(1)} %get-tuple-element.23), channel_id=1, source_target_pairs={{0,2},{2,4},{4,6},{6,8},{8,10},{10,12},{12,14},{14,16},{16,18},{18... | collective-permute-start | bytes 196616 | tf_op jit(solution)/shard_map/ppermute | solution.py:17
  24.8 4.4 %collective-permute-start.1 = (bf16[128,256]{1,0:T(8,128)(2,1)S(1)}, bf16[128,256]{1,0:T(8,128)(2,1)S(1)}, u32[]{:S(2)}, u32[]{:S(2)}) collective-permute-start(bf16[128,256]{1,0:T(8,128)(2,1)S(1)} %get-tuple-element.24), channel_id=1, source_target_pairs={{2,0},{4,2},{6,4},{8,6},{10,8},{12,10},{14,12},{16,14},{18,16},{20... | collective-permute-start | bytes 196616 | tf_op jit(solution)/shard_map/ppermute | solution.py:17
  34.5 10.0 %copy-start.1 = (bf16[256,2048]{1,0:T(8,128)(2,1)S(1)}, bf16[256,2048]{1,0:T(8,128)(2,1)}, u32[]{:S(2)}) copy-start(bf16[256,2048]{1,0:T(8,128)(2,1)} %param.17) | copy-start | bytes 3145732
  48.1 0.7 copy-start.4
  50.1 186.5 %all-gather.8.cloned.1.call-start = ((), (), s32[]{:S(2)}) async-start(), calls=%async_computation.3 | async-start | bytes 12255232 | tf_op jit(solution)/shard_map/all_gather | solution.py:92
  50.9 280.2 %all-gather.10.cloned.1.call-start = ((), (), s32[]{:S(2)}) async-start(), calls=%async_computation.4 | async-start | bytes 12255232 | tf_op jit(solution)/shard_map/all_gather | solution.py:93
  51.4 337.1 %reduce-scatter.2.cloned.1.call-start = ((), (), s32[]{:S(2)}) async-start(), calls=%async_computation.5 | async-start | bytes 3145728 | tf_op jit(solution)/shard_map/reduce_scatter | solution.py:104
  388.5 2.0 copy-start
  390.4 0.8 copy-start.6
Sparse Core Ops, SparseCore 0:
  9.6 97.7 all-gather.11
  109.0 31.3 all-gather.5
  142.6 93.9 all-gather.7
  238.8 92.2 all-gather.9
  358.4 30.0 reduce-scatter.1
